TPU v7x, 256 devices: a 4x2x16 block of a 4x16x16 slice. The times are simulated.
256 devices in a mesh: grp: 2 (over y), st: 32 (over z, core), tp: 4 (over x).
Axes of the slice: x: 4, y: 2, z: 16, core: 2. Of those that a mesh axis runs over, the one named last changes fastest.
The devices are a block of a 4x16x16 slice.
Arguments:
- tokens: bfloat16 [65536, 2048], P(('grp', 'st'), 'tp'), parts along dimension 0, may hold values from -6 to 6
- norm_gain: float32 [2048], replicated, may hold values from 0.1 to 1.9
- pool_weight: bfloat16 [4, 512, 512], P('tp'), may hold values from -0.25 to 0.25
- pool_scale: float32 [2048], P('tp'), may hold values from 0.1 to 1.9
- query_weight: bfloat16 [2048, 1024], P(None, 'tp'), may hold values from -3 to 3
- gate_weight: bfloat16 [2048, 8], replicated, may hold values from -0.125 to 0.125
- key_weight: bfloat16 [2048, 1024], P(None, 'tp'), may hold values from -0.125 to 0.125
- value_weight: bfloat16 [2048, 1024], P(None, 'tp'), may hold values from -0.125 to 0.125
- out_weight: bfloat16 [1024, 2048], P(None, 'tp'), may hold values from -0.1875 to 0.1875
- passage_gain: float32 [2048], replicated, may hold values from 0.1 to 1.9
- passage_store: bfloat16 [1536, 64, 2048], P(('grp', 'st')), parts along dimension 0, may hold values from -6 to 6
- passage_ids: int32 [512, 4], P(('grp', 'st')), parts along dimension 0, may hold values from 0 to 767, as said below
Outputs:
- mixed: bfloat16 [65536, 2048], P(('grp', 'st'), 'tp'), parts along dimension 0
There are 2 independent parts, one for each index of `grp`. A program takes and returns all parts, laid end to end along the dimension named above; an argument that names none is the same for every part. Nothing has to cross between parts.
Inputs may be any that keep to these rules, and one draw needn't show every extreme that they name: `passage_ids`: the ids of the blocks of one index of st name at most 2 passages held by any one index of st, and exactly 2 held by some index.
All inputs are finite; a program needn't handle non-finite values.
Results may differ from a plain program's by a relative error of at most 0.009.
Values may be sent and summed in bfloat16 or wider, within the bound.
A program may use at most 128 MiB of HBM per device.

v0:
```python
import jax
import jax.numpy as jnp
from jax import lax
from jax.sharding import PartitionSpec as P

HD = 128
GROUPS = 4
SEQ_LEN = 256
BLK = 128
NPB = 4
PLEN = 64
P_DEV = 24


epsilon = 1e-06


def in_order(pieces, dim):
    lengths = list(pieces.shape[1:])
    lengths[dim] *= pieces.shape[0]
    return jnp.moveaxis(pieces, 0, dim).reshape(lengths)


def copy_for_each(value, axis):
    copies = jnp.broadcast_to(value, (lax.axis_size(axis), *value.shape))
    return lax.all_to_all(copies, axis, split_axis=0, concat_axis=0, tiled=True)


def gather_directly(value, axis, dim):
    return in_order(copy_for_each(value, axis), dim)


def normalize_rows(fetched, passage_gain):
    wide_rows = fetched.astype(jnp.float32)
    inverse = lax.rsqrt(jnp.mean(wide_rows * wide_rows, axis=-1, keepdims=True) + epsilon)
    return (wide_rows * inverse * passage_gain).astype(jnp.bfloat16)


def project_rows(fetched, passage_gain, both_weights):
    count_rows = fetched.shape[0]
    flat_rows = normalize_rows(fetched.reshape(count_rows * PLEN, fetched.shape[2]), passage_gain)
    projected = jnp.dot(flat_rows, both_weights, preferred_element_type=jnp.float32).astype(
        jnp.bfloat16
    )
    return projected.reshape(count_rows, PLEN, both_weights.shape[1])


def per_device(
    tokens,
    norm_gain,
    pool_weight,
    pool_scale,
    query_weight,
    gate_weight,
    key_weight,
    value_weight,
    out_weight,
    passage_gain,
    passage_store,
    passage_ids,
):
    head_index = lax.axis_index("tp")
    tok_rows, width_local = tokens.shape
    full_width = width_local * lax.axis_size("tp")
    local_heads = query_weight.shape[1] // HD
    head_width = local_heads * HD
    wide_tokens = tokens.astype(jnp.float32)
    square_sums = lax.psum(jnp.sum(wide_tokens * wide_tokens, axis=1), "tp")
    inverse = lax.rsqrt(square_sums / full_width + epsilon)
    gain_local = lax.dynamic_slice_in_dim(norm_gain, head_index * width_local, width_local)
    normed = (wide_tokens * inverse[:, None] * gain_local[None, :]).astype(jnp.bfloat16)
    sequences = tok_rows // SEQ_LEN
    widest = 2**GROUPS
    window = jnp.left_shift(jnp.int32(2), head_index)
    grouped = normed.astype(jnp.float32).reshape(sequences, SEQ_LEN, width_local)
    running = jnp.cumsum(grouped, axis=1)
    padded = jnp.concatenate(
        [jnp.zeros((sequences, widest, width_local), jnp.float32), running], axis=1
    )
    lagged = lax.dynamic_slice_in_dim(padded, widest - window, SEQ_LEN, axis=1)
    position = jnp.arange(SEQ_LEN, dtype=jnp.int32)
    divisor = jnp.minimum(position + 1, window).astype(jnp.float32)
    pooled = (
        ((running - lagged) / divisor[None, :, None] - grouped)
        .astype(jnp.bfloat16)
        .reshape(tok_rows, width_local)
    )
    mixing = (
        jnp.dot(pooled, pool_weight[0], preferred_element_type=jnp.float32) * pool_scale[None, :]
    )
    gate_columns = lax.dynamic_slice_in_dim(
        gate_weight, head_index * local_heads, local_heads, axis=1
    )
    columns = lax.all_gather(normed, "tp", axis=1, tiled=True)
    query_sum = jnp.dot(columns, query_weight, preferred_element_type=jnp.float32)
    gate_sum = jnp.dot(columns, gate_columns, preferred_element_type=jnp.float32)
    queries = query_sum.astype(jnp.bfloat16)
    gating = jax.nn.sigmoid(gate_sum)
    flat_ids = passage_ids.reshape(-1)
    asked_count = flat_ids.shape[0]
    st_count = lax.axis_size("st")
    capacity = max(2, (asked_count + st_count - 1) // st_count)
    owners = flat_ids // P_DEV
    local_index = flat_ids % P_DEV
    order_index = jnp.arange(asked_count, dtype=jnp.int32)
    earlier = (owners[None, :] == owners[:, None]) & (order_index[None, :] < order_index[:, None])
    slot_index = jnp.sum(earlier.astype(jnp.int32), axis=1)
    position_flat = owners * capacity + slot_index
    slot_range = jnp.arange(st_count * capacity, dtype=jnp.int32)
    request_table = jnp.sum(
        jnp.where(position_flat[None, :] == slot_range[:, None], local_index[None, :], 0), axis=1
    )
    request_table = request_table.reshape(st_count, capacity)
    asked = lax.all_to_all(request_table, "st", split_axis=0, concat_axis=0, tiled=True)
    both_weights = jnp.concatenate([key_weight, value_weight], axis=1)
    projected_store = project_rows(passage_store, passage_gain, both_weights)
    projected = jnp.take(projected_store, asked.reshape(-1), axis=0)
    returned = lax.all_to_all(
        projected.reshape(st_count, capacity * PLEN, 2 * head_width),
        "st",
        split_axis=0,
        concat_axis=0,
        tiled=True,
    )
    key_values = jnp.take(
        returned.reshape(st_count * capacity, PLEN, 2 * head_width), position_flat, axis=0
    )
    block_count = tok_rows // BLK
    key_values = key_values.reshape(block_count, NPB * PLEN, 2 * head_width)
    key_rows = key_values[:, :, :head_width].reshape(block_count, NPB * PLEN, local_heads, HD)
    values = key_values[:, :, head_width:].reshape(block_count, NPB * PLEN, local_heads, HD)
    query_blocks = queries.reshape(block_count, BLK, local_heads, HD)
    scores = jnp.einsum(
        "bqhd,bkhd->bhqk", query_blocks, key_rows, preferred_element_type=jnp.float32
    ) * HD ** (-0.5)
    row_max = jnp.max(scores, axis=-1, keepdims=True)
    weights = jnp.exp(scores - row_max)
    probabilities = (weights / jnp.sum(weights, axis=-1, keepdims=True)).astype(jnp.bfloat16)
    attended = jnp.einsum(
        "bhqk,bkhd->bqhd", probabilities, values, preferred_element_type=jnp.float32
    ).reshape(tok_rows, local_heads, HD)
    head_out = (attended * gating[:, :, None]).astype(jnp.bfloat16).reshape(tok_rows, head_width)
    crossed = jnp.dot(
        gather_directly(head_out, "tp", 1), out_weight, preferred_element_type=jnp.float32
    )
    return (mixing + crossed).astype(jnp.bfloat16)


def solution(mesh):
    in_specs = (
        P(("grp", "st"), "tp"),
        P(),
        P("tp", None, None),
        P("tp"),
        P(None, "tp"),
        P(),
        P(None, "tp"),
        P(None, "tp"),
        P(None, "tp"),
        P(),
        P(("grp", "st"), None, None),
        P(("grp", "st"), None),
    )
    out_specs = P(("grp", "st"), "tp")
    return jax.shard_map(
        per_device, mesh=mesh, in_specs=in_specs, out_specs=out_specs, check_vma=False
    )
```

profile of v0, /device:TPU:40, one launch (start us, length us, event | category | flops | bytes accessed | tf_op | source)
XLA Modules:
  0.0 312.0 jit_solution(15482940754100980256)
XLA Ops:
  6.6 0.8 copy.47
  7.7 0.2 convert_reduce_fusion
  7.9 0.1 select_reduce_fusion
  8.0 0.7 all_to_all.12
  8.7 24.7 %all-to-all-start = ((s32[32,1,2]{2,1,0:T(1,128)}), s32[32,1,2]{2,1,0:T(1,128)S(1)}, u32[]{:S(2)}, u32[]{:S(2)}) async-start(s32[32,1,2]{2,1,0:T(1,128)} %bitcast.9), calls=%async_computation | async-start | bytes 32768 | tf_op jit(solution)/shard_map/all_to_all | solution.py:114
  33.4 4.1 %multiply_reduce_fusion = f32[24,64]{1,0:T(8,128)S(1)} fusion(bf16[24,64,2048]{2,1,0:T(8,128)(2,1)} %param.22), kind=kLoop, calls=%fused_computation.6 | loop fusion | flops 9435648 | bytes 6297600 | tf_op jit(solution)/shard_map/reduce_sum | solution.py:35
  37.6 4.4 %fusion.2 = bf16[1536,2048]{1,0:T(8,128)(2,1)S(1)} fusion(f32[2048]{0:T(1024)S(1)} %copy-done.5, f32[1536]{0:T(1024)S(1)} %rsqrt.16, bf16[24,64,2048]{2,1,0:T(8,128)(2,1)} %param.22), kind=kLoop, calls=%fused_computation.5 | loop fusion | flops 12582912 | bytes 12597248 | tf_op jit(solution)/shard_map/convert_element_type | solution.py:36
  42.1 3.5 %convolution_convert_fusion = bf16[1536,512]{1,0:T(8,128)(2,1)S(1)} fusion(bf16[1536,2048]{1,0:T(8,128)(2,1)S(1)} %fusion.2, bf16[2048,256]{1,0:T(8,128)(2,1)S(1)} %copy-done.7, bf16[2048,256]{1,0:T(8,128)(2,1)S(1)} %copy-done.8), kind=kOutput, calls=%fused_computation.8 | convolution fusion | flops 3226206208 | bytes 9961472 | tf_op jit(solution)/shard_map/dot_general | solution.py:42
  45.7 0.1 copy.52
  45.8 0.1 broadcast_in_dim.65
  46.0 0.1 broadcast_in_dim.66
  46.0 0.5 broadcast.275
  46.6 0.7 reduce.4
  47.3 0.1 reshape.270
  47.4 2.8 gather_fusion
  50.2 3.9 %bitcast_select_fusion = bf16[32,128,512]{2,1,0:T(8,128)(2,1)} fusion(pred[32,128]{1,0:T(8,128)(4,1)S(1)} %broadcast_in_dim.66, bf16[32,128,512]{2,1,0:T(8,128)(2,1)} %bitcast.68), kind=kLoop, calls=%fused_computation.7 | loop fusion | flops 2097152 | bytes 8392704 | tf_op jit(solution)/shard_map/jit(_take)/select_n | solution.py:117
  54.0 12.6 %all-to-all-start.1 = ((bf16[32,128,512]{2,1,0:T(8,128)(2,1)}), bf16[32,128,512]{2,1,0:T(8,128)(2,1)}, u32[]{:S(2)}, u32[]{:S(2)}) async-start(bf16[32,128,512]{2,1,0:T(8,128)(2,1)} %bitcast_select_fusion), calls=%async_computation.1 | async-start | bytes 8388608 | tf_op jit(solution)/shard_map/all_to_all | solution.py:118
  66.7 0.8 dynamic_slice.9
  67.4 0.3 fusion.6
  67.7 10.9 %psum.7 = f32[1024]{0:T(1024)S(1)} all-reduce(f32[1024]{0:T(1024)S(1)} %fusion.6), channel_id=1, replica_groups=mesh['grp'=2,'st'=32,'tp'=4] {'tp'}, use_global_device_ids=true, to_apply=%region_1.0 | all-reduce | flops 1024 | bytes 8192 | tf_op jit(solution)/shard_map/psum | solution.py:68
  78.7 1.4 fusion.8
  80.4 0.1 broadcast_in_dim.61
  80.6 52.4 %all-gather.2.cloned.1.call-done = bf16[1024,2048]{1,0:T(8,128)(2,1)} async-done(((bf16[1024,512]{1,0:T(8,128)(2,1)}), bf16[1024,2048]{1,0:T(8,128)(2,1)}) %all-gather.2.cloned.1.call-update) | async-done | bytes 4194320 | tf_op jit(solution)/shard_map/all_gather | solution.py:94
  133.0 3.7 %convolution_convert_fusion.1 = bf16[1024,256]{1,0:T(8,128)(2,1)S(1)} fusion(bf16[1024,2048]{1,0:T(8,128)(2,1)} %all-gather.2.cloned.1.call-done, bf16[2048,256]{1,0:T(8,128)(2,1)} %param.16), kind=kOutput, calls=%fused_computation.31 | convolution fusion | flops 1074003968 | bytes 5767168 | tf_op jit(solution)/shard_map/dot_general | solution.py:95
  136.7 0.9 reshape.273
  137.6 3.4 %fusion.18 = f32[1024,2]{0,1:T(2,128)S(1)} fusion(bf16[1024,2048]{1,0:T(8,128)(2,1)} %all-gather.2.cloned.1.call-done, bf16[2048,8]{0,1:T(8,128)(2,1)} %param.17, s32[]{:T(128)S(6)} %select_n.109), kind=kOutput, calls=%fused_computation.35 | convolution fusion | flops 8394752 | bytes 4210692 | tf_op jit(solution)/shard_map/dot_general | solution.py:96
  141.0 109.1 %all-to-all-done.1 = bf16[32,128,512]{2,1,0:T(8,128)(2,1)} async-done(((bf16[32,128,512]{2,1,0:T(8,128)(2,1)}), bf16[32,128,512]{2,1,0:T(8,128)(2,1)}, u32[]{:S(2)}, u32[]{:S(2)}) %all-to-all-start.1) | async-done | bytes 4194336 | tf_op jit(solution)/shard_map/all_to_all | solution.py:118
  250.1 2.9 gather_fusion.1
  253.0 0.5 bitcast_select_fusion.1
  253.4 1.2 fusion.46
  254.6 1.5 copy.54
  256.1 2.0 fusion.47
  258.1 2.8 fusion.22
  260.9 0.5 copy.53
  261.5 5.3 %convolution_bitcast_fusion = f32[8,128,2,128]{1,3,2,0:T(8,128)S(1)} fusion(bf16[8,256,2,128]{1,3,2,0:T(8,128)(2,1)S(1)} %bitcast.77, f32[8,2,128]{2,1,0:T(2,128)S(1)} %fusion.47, f32[8,2,128,256]{3,2,1,0:T(8,128)} %fusion.22), kind=kOutput, calls=%fused_computation.30 | convolution fusion | flops 136317184 | bytes 4202496 | tf_op jit(solution)/shard_map/bhqk,bkhd->bqhd/dot_general | solution.py:139
  266.8 0.6 copy.57
  267.4 0.2 fusion.19
  267.6 1.6 broadcast_in_dim.70
  269.2 4.9 %all-to-all-start.2 = ((bf16[4,1024,256]{1,2,0:T(8,128)(2,1)}), bf16[4,1024,256]{1,2,0:T(8,128)(2,1)}, u32[]{:S(2)}, u32[]{:S(2)}) async-start(bf16[4,1024,256]{1,2,0:T(8,128)(2,1)} %broadcast_in_dim.70), calls=%async_computation.2 | async-start | bytes 4194304 | tf_op jit(solution)/shard_map/all_to_all | solution.py:26
  274.1 0.3 convert.2
  274.4 1.6 fusion.12
  276.1 1.3 copy-done.2
  277.5 2.3 broadcast_add_fusion
  279.8 1.7 copy.46
  281.5 3.1 fusion.14
  284.6 15.9 %all-to-all-done.2 = bf16[4,1024,256]{1,2,0:T(8,128)(2,1)} async-done(((bf16[4,1024,256]{1,2,0:T(8,128)(2,1)}), bf16[4,1024,256]{1,2,0:T(8,128)(2,1)}, u32[]{:S(2)}, u32[]{:S(2)}) %all-to-all-start.2) | async-done | bytes 2097184 | tf_op jit(solution)/shard_map/all_to_all | solution.py:26
  300.4 2.9 fusion.50
  303.4 1.7 add_convert_fusion
  (45 shorter events, 1.0 us)
Async XLA Ops:
  6.5 293.9 %copy-start = (bf16[1024,512]{1,0:T(8,128)(2,1)S(1)}, bf16[1024,512]{1,0:T(8,128)(2,1)}, u32[]{:S(2)}) copy-start(bf16[1024,512]{1,0:T(8,128)(2,1)} %param.20) | copy-start | bytes 3145732
  8.7 37.0 %all-to-all-start = ((s32[32,1,2]{2,1,0:T(1,128)}), s32[32,1,2]{2,1,0:T(1,128)S(1)}, u32[]{:S(2)}, u32[]{:S(2)}) async-start(s32[32,1,2]{2,1,0:T(1,128)} %bitcast.9), calls=%async_computation | async-start | bytes 32768 | tf_op jit(solution)/shard_map/all_to_all | solution.py:114
  33.4 4.2 %copy-start.5 = (f32[2048]{0:T(1024)S(1)}, f32[2048]{0:T(1024)}, u32[]{:S(2)}) copy-start(f32[2048]{0:T(1024)} %param.21) | copy-start | bytes 24580
  37.6 4.4 %copy-start.7 = (bf16[2048,256]{1,0:T(8,128)(2,1)S(1)}, bf16[2048,256]{1,0:T(8,128)(2,1)}, u32[]{:S(2)}) copy-start(bf16[2048,256]{1,0:T(8,128)(2,1)} %param.19) | copy-start | bytes 3145732
  37.6 4.5 %copy-start.8 = (bf16[2048,256]{1,0:T(8,128)(2,1)S(1)}, bf16[2048,256]{1,0:T(8,128)(2,1)}, u32[]{:S(2)}) copy-start(bf16[2048,256]{1,0:T(8,128)(2,1)} %param.18) | copy-start | bytes 3145732
  54.0 13.4 %copy-start.3 = (bf16[1024,512]{1,0:T(8,128)(2,1)S(1)}, bf16[1024,512]{1,0:T(8,128)(2,1)}, u32[]{:S(2)}) copy-start(bf16[1024,512]{1,0:T(8,128)(2,1)} %param.12) | copy-start | bytes 3145732
  54.0 196.0 %all-to-all-start.1 = ((bf16[32,128,512]{2,1,0:T(8,128)(2,1)}), bf16[32,128,512]{2,1,0:T(8,128)(2,1)}, u32[]{:S(2)}, u32[]{:S(2)}) async-start(bf16[32,128,512]{2,1,0:T(8,128)(2,1)} %bitcast_select_fusion), calls=%async_computation.1 | async-start | bytes 8388608 | tf_op jit(solution)/shard_map/all_to_all | solution.py:118
  66.6 66.4 %all-gather.2.cloned.1.call-start = ((), (), s32[]{:S(2)}) async-start(), calls=%async_computation.3 | async-start | bytes 5242880 | tf_op jit(solution)/shard_map/all_gather | solution.py:94
  269.2 4.9 %copy-start.1 = (bf16[1024,512]{1,0:T(8,128)(2,1)S(1)}, bf16[1024,512]{1,0:T(8,128)(2,1)}, u32[]{:S(2)}) copy-start(bf16[1024,512]{1,0:T(8,128)(2,1)} %fusion.8) | copy-start | bytes 3145732
  269.2 31.2 %all-to-all-start.2 = ((bf16[4,1024,256]{1,2,0:T(8,128)(2,1)}), bf16[4,1024,256]{1,2,0:T(8,128)(2,1)}, u32[]{:S(2)}, u32[]{:S(2)}) async-start(bf16[4,1024,256]{1,2,0:T(8,128)(2,1)} %broadcast_in_dim.70), calls=%async_computation.2 | async-start | bytes 4194304 | tf_op jit(solution)/shard_map/all_to_all | solution.py:26
  276.0 1.3 copy-start.2
  300.4 2.9 copy-start.4
  300.4 2.9 copy-start.6
Sparse Core Ops, SparseCore 0:
  80.2 52.6 all-gather.1
where the time goes:
time: 316 us; the launch traced here: 312 us
  waiting for transfers between devices  177 us (56%)
  starting transfers between devices  42.2 us (13%)
  matrix products  25.5 us (8%)
  other arithmetic  23.1 us (7%)
  local copies, waits for them, and re-layouts  19.1 us (6%)
  between operations  13.7 us (4%)
  blocking collectives  10.9 us (3%)
    all_to_all x1, waiting for transfers between devices, per_device(): lax.all_to_all(projected.reshape(st_count, capacity * PLEN, 2 * head_widt...  109 us
    all_gather x1, waiting for transfers between devices, per_device(): columns = lax.all_gather(normed, 'tp', axis=1, tiled=True)  52.4 us
    all_to_all x1, starting transfers between devices, per_device(): lax.all_to_all(request_table, 'st', split_axis=0, concat_axis=0, tiled=True)  24.7 us
    all_to_all x1, waiting for transfers between devices, copy_for_each(): return lax.all_to_all(copies, axis, split_axis=0, concat_axis=0, tiled=True)  15.9 us
    all_to_all x1, starting transfers between devices, per_device(): lax.all_to_all(projected.reshape(st_count, capacity * PLEN, 2 * head_widt...  12.6 us
    psum x1, blocking collectives, per_device(): square_sums = lax.psum(jnp.sum(wide_tokens * wide_tokens, axis=1), 'tp')  10.9 us
  transfers between devices with their start and end apart: 4, of which 3 were waited for; matrix products, arithmetic and copies ran while one was open for 10% of the time, Pallas kernels for 0%

commit v1 on v0

v1 whole, which is shorter than its diff:
```python
import functools

import jax
import jax.numpy as jnp
from jax import lax
from jax.experimental import pallas as pl
from jax.experimental.pallas import tpu as pltpu
from jax.sharding import PartitionSpec as P

HD = 128
GROUPS = 4
SEQ_LEN = 256
BLK = 128
NPB = 4
PLEN = 64
P_DEV = 24
CORES = 2
CHIP_PASSAGES = CORES * P_DEV

LAG = 4
LAND = 16
STAGE = 6
MOST_ROUNDS = 128
LEVELS = (72, 75, 78, 82, 90)

epsilon = 1e-06
MESH = pl.DeviceIdType.MESH


def project_kernel(ids_ref, gain_ref, key_ref, value_ref, store_ref, ring_ref, both_ref,
                   buf, load_sem, id_send, id_recv, kv_send, kv_recv):
    me = lax.axis_index("st")
    count = lax.axis_size("st")
    chips = count // CORES
    core = me % CORES
    chip = me // CORES
    partner = chip * CORES + (1 - core)
    barrier = pltpu.get_barrier_semaphore()
    pl.semaphore_signal(barrier, inc=1, device_id={"st": partner}, device_id_type=MESH)
    for step in range(1, chips):
        peer = lax.rem(chip + step, chips) * CORES + core
        pl.semaphore_signal(barrier, inc=1, device_id={"st": peer}, device_id_type=MESH)
    per = buf.shape[1]
    chunks = P_DEV // per
    rows = per * PLEN

    def load(index):
        return pltpu.make_async_copy(
            store_ref.at[pl.ds(index * per, per)], buf.at[index % 2], load_sem.at[index % 2])

    def give(index):
        there = both_ref.at[core, pl.ds(index * per, per)]
        return pltpu.make_async_remote_copy(
            src_ref=there, dst_ref=there, send_sem=kv_send.at[index], recv_sem=kv_recv.at[index],
            device_id={"st": partner}, device_id_type=MESH)

    def tell(step):
        peer = lax.rem(chip + step, chips) * CORES + core
        return pltpu.make_async_remote_copy(
            src_ref=ids_ref, dst_ref=ring_ref.at[chip],
            send_sem=id_send.at[step], recv_sem=id_recv.at[step],
            device_id={"st": peer}, device_id_type=MESH)

    load(0).start()
    ring_ref[chip] = ids_ref[...]
    for index in range(chunks):
        if index + 1 < chunks:
            load(index + 1).start()
        load(index).wait()
        if index == 1:
            pl.semaphore_wait(barrier, chips)
            for step in range(1, chips):
                tell(step).start()
        wide = buf[index % 2].astype(jnp.float32).reshape(rows, buf.shape[3])
        inverse = lax.rsqrt(jnp.mean(wide * wide, axis=-1, keepdims=True) + epsilon)
        normed = (wide * inverse * gain_ref[...]).astype(jnp.bfloat16)
        width = key_ref.shape[1]
        keys = jnp.dot(normed, key_ref[...], preferred_element_type=jnp.float32)
        values = jnp.dot(normed, value_ref[...], preferred_element_type=jnp.float32)
        own = pl.ds(index * per, per)
        both_ref[core, own, :, :width] = keys.astype(jnp.bfloat16).reshape(per, PLEN, width)
        both_ref[core, own, :, width:] = values.astype(jnp.bfloat16).reshape(per, PLEN, width)
        if index >= 2:
            give(index - 1).start()
        if index == 1:
            give(0).start()
    for step in range(1, chips):
        tell(step).wait()
    give(chunks - 1).start()
    for index in range(chunks):
        give(index).wait()


def project(ids_row, passage_gain, key_weight, value_weight, passage_store, chips):
    width = key_weight.shape[1] + value_weight.shape[1]
    per = 4
    vmem = pl.BlockSpec(memory_space=pltpu.VMEM)
    rows = passage_store.shape[0] * PLEN
    return pl.pallas_call(
        project_kernel,
        name="project_kernel",
        out_shape=(
            jax.ShapeDtypeStruct((chips, 1, ids_row.shape[1]), jnp.int32),
            jax.ShapeDtypeStruct((CORES, P_DEV, PLEN, width), jnp.bfloat16),
        ),
        in_specs=[vmem] * 4 + [pl.BlockSpec(memory_space=pl.ANY)],
        out_specs=(vmem, vmem),
        scratch_shapes=[
            pltpu.VMEM((2, per, PLEN, passage_store.shape[2]), jnp.bfloat16),
            pltpu.SemaphoreType.DMA((2,)),
            pltpu.SemaphoreType.DMA((chips,)),
            pltpu.SemaphoreType.DMA((chips,)),
            pltpu.SemaphoreType.DMA((P_DEV // per,)),
            pltpu.SemaphoreType.DMA((P_DEV // per,)),
        ],
        cost_estimate=pl.CostEstimate(
            flops=2 * rows * passage_store.shape[2] * width,
            bytes_accessed=2 * rows * (passage_store.shape[2] + width),
            transcendentals=0),
        compiler_params=pltpu.CompilerParams(collective_id=0, has_side_effects=True),
    )(ids_row, passage_gain[None, :], key_weight, value_weight, passage_store)


def plan(ring_ids, chip):
    chips = ring_ids.shape[0]
    half = chips // 2
    reads = ring_ids.shape[1]
    source = ring_ids // CHIP_PASSAGES
    passage = ring_ids % CHIP_PASSAGES
    reader = lax.broadcasted_iota(jnp.int32, source.shape, 0)
    order = jnp.arange(reads, dtype=jnp.int32)
    same = (source[:, :, None] == source[:, None, :]) & (order[None, None, :] < order[None, :, None])
    before = jnp.sum(same.astype(jnp.int32), axis=2)
    around = (reader - source + chips) % chips
    turn = (before + reader) % 2
    is_up = ((around >= 1) & (around < half)) | ((around == half) & (turn == 0))
    is_down = (around > half) | ((around == half) & (turn == 1))
    going = jnp.stack([is_up, is_down])
    distance = jnp.stack([around, (chips - around) % chips])
    start = jnp.stack([source, (chips - source) % chips])
    place = jnp.where(around == half, before // 2, before)
    here = jnp.stack([chip, (chips - chip) % chips])
    node = jnp.arange(chips, dtype=jnp.int32)
    hop = jnp.arange(half, dtype=jnp.int32)
    counted = (
        going[:, None, None]
        & (start[:, None, None] == node[None, :, None, None, None])
        & (distance[:, None, None] > hop[None, None, :, None, None])
    )
    further = jnp.sum(counted.astype(jnp.int32), axis=(3, 4))
    starts = [jnp.zeros((2, chips), jnp.int32)]
    for j in range(1, half):
        starts.append(jnp.maximum(
            jnp.roll(starts[-1] + further[:, :, j - 1], -1, axis=1), starts[-1] + LAG))
    begin = jnp.stack(starts, axis=2)
    rounds = jnp.max(jnp.where(further > 0, begin + further, 0))
    upstream = (here[:, None] - hop[None, :] + chips) % chips
    chosen = (node[None, :, None] == upstream[:, None, :]).astype(jnp.int32)
    opens = jnp.sum(chosen * begin, axis=1)
    lengths = jnp.sum(chosen * further, axis=1)
    shifted = jnp.concatenate([jnp.zeros_like(begin[:, :, :1]), begin[:, :, :-1]], axis=2)
    arrived = jnp.sum(chosen * shifted, axis=1)
    clock = jnp.arange(MOST_ROUNDS, dtype=jnp.int32)[None, :, None]
    lane = jnp.arange(2, dtype=jnp.int32)
    active = (
        (clock >= opens[:, None]) & (clock < (opens + lengths)[:, None]) & (hop[None, None] > 0)
    )
    passing = jnp.sum(
        jnp.where(active, CHIP_PASSAGES + lane[:, None, None] + 2 * (arrived[:, None] + clock - opens[:, None]), 0),
        axis=2)
    further_padded = jnp.concatenate([further, jnp.zeros_like(further[:, :, :1])], axis=2)
    steps = jnp.arange(half + 1, dtype=jnp.int32)
    own_further = jnp.sum(
        jnp.where(node[None, :, None] == here[:, None, None], further_padded, 0), axis=1)
    position = place + jnp.sum(
        jnp.where(distance[..., None] == steps, own_further[:, None, None, :], 0), axis=3)
    leaving = going & (source == chip)
    first = jnp.sum(
        jnp.where(leaving[:, None] & (position[:, None] == clock[:, :, :, None]), passage, 0),
        axis=(2, 3))
    sends = passing + first
    row = lax.dynamic_slice_in_dim
    my_going = row(going, chip, 1, axis=1)[:, 0]
    my_start = row(start, chip, 1, axis=1)[:, 0]
    my_distance = row(distance, chip, 1, axis=1)[:, 0]
    my_place = row(place, chip, 1, axis=0)[0]
    my_passage = row(passage, chip, 1, axis=0)[0]
    last = begin + further_padded[:, :, 1:]
    picked = (
        (my_start[:, :, None, None] == node[None, None, :, None])
        & (my_distance[:, :, None, None] == hop[None, None, None, :] + 1)
    )
    arrival = jnp.sum(jnp.where(picked, last[:, None], 0), axis=(2, 3)) + my_place
    lands = jnp.sum(jnp.where(my_going, CHIP_PASSAGES + lane[:, None] + 2 * arrival, 0), axis=0)
    lands = jnp.where(my_going[0] | my_going[1], lands, my_passage)
    table = jnp.concatenate([sends, jnp.pad(lands, (0, MOST_ROUNDS - reads))[None]], axis=0)
    return table, rounds


def ring_kernel(rounds, table_ref, kept_ref, out_ref, pool, land, stage, send_sem, recv_sem):
    me = lax.axis_index("st")
    count = lax.axis_size("st")
    up = lax.rem(me + CORES, count)
    down = lax.rem(me + count - CORES, count)
    target = (up, down)
    barrier = pltpu.get_barrier_semaphore()
    for peer in target:
        pl.semaphore_signal(barrier, inc=1, device_id={"st": peer}, device_id_type=MESH)
    pool[:CHIP_PASSAGES] = kept_ref[...]
    pl.semaphore_wait(barrier, 2)

    def copy(way, index):
        return pltpu.make_async_remote_copy(
            src_ref=stage.at[way, index % STAGE], dst_ref=land.at[way, index % LAND],
            send_sem=send_sem.at[way, index % STAGE], recv_sem=recv_sem.at[way, index % LAND],
            device_id={"st": target[way]}, device_id_type=MESH)

    def put(way, index):
        stage[way, index % STAGE] = pool[table_ref[way, index]]

    def take(way, index):
        pool[CHIP_PASSAGES + 2 * index + way] = land[way, index % LAND]

    def one_round(index, fresh, arriving, sending):
        if arriving:
            for way in range(2):
                copy(way, index - LAG).wait_recv()
        if sending:
            for way in range(2):
                copy(way, index - 1).start()
        if arriving:
            for way in range(2):
                take(way, index - LAG)
        if fresh:
            for way in range(2):
                put(way, index)

    for index in range(LAG):
        one_round(index, True, False, index >= 1)

    def middle(index, carry):
        @pl.when(index >= STAGE)
        def _():
            for way in range(2):
                copy(way, index - STAGE).wait_send()
        one_round(index, True, True, True)
        return carry

    lax.fori_loop(LAG, rounds, middle, 0)
    for index in range(rounds, rounds + LAG):
        one_round(index, False, True, index == rounds)
    for index in range(rounds - STAGE, rounds):
        for way in range(2):
            copy(way, index).wait_send()

    def hand(index, carry):
        out_ref[index] = pool[table_ref[2, index]]
        return carry

    lax.fori_loop(0, out_ref.shape[0], hand, 0)


def ring(rounds, ident, reads, table, kept):
    slot = kept.shape[1:]
    vmem = pl.BlockSpec(memory_space=pltpu.VMEM)
    size = slot[0] * slot[1]
    return pl.pallas_call(
        functools.partial(ring_kernel, rounds),
        name=f"ring_kernel_{rounds}",
        out_shape=jax.ShapeDtypeStruct((reads, *slot), jnp.bfloat16),
        in_specs=[pl.BlockSpec(memory_space=pltpu.SMEM), vmem],
        out_specs=vmem,
        scratch_shapes=[
            pltpu.VMEM((CHIP_PASSAGES + 2 * rounds, *slot), jnp.bfloat16),
            pltpu.VMEM((2, LAND, *slot), jnp.bfloat16),
            pltpu.VMEM((2, STAGE, *slot), jnp.bfloat16),
            pltpu.SemaphoreType.DMA((2, STAGE)),
            pltpu.SemaphoreType.DMA((2, LAND)),
        ],
        cost_estimate=pl.CostEstimate(
            flops=rounds * 10**9, bytes_accessed=rounds * size * 8, transcendentals=0),
        compiler_params=pltpu.CompilerParams(collective_id=ident, has_side_effects=True),
    )(table, kept)


def per_device(
    tokens,
    norm_gain,
    pool_weight,
    pool_scale,
    query_weight,
    gate_weight,
    key_weight,
    value_weight,
    out_weight,
    passage_gain,
    passage_store,
    passage_ids,
):
    head_index = lax.axis_index("tp")
    tok_rows, width_local = tokens.shape
    full_width = width_local * lax.axis_size("tp")
    local_heads = query_weight.shape[1] // HD
    head_width = local_heads * HD
    wide_tokens = tokens.astype(jnp.float32)
    square_sums = lax.psum(jnp.sum(wide_tokens * wide_tokens, axis=1), "tp")
    inverse = lax.rsqrt(square_sums / full_width + epsilon)
    gain_local = lax.dynamic_slice_in_dim(norm_gain, head_index * width_local, width_local)
    normed = (wide_tokens * inverse[:, None] * gain_local[None, :]).astype(jnp.bfloat16)
    sequences = tok_rows // SEQ_LEN
    widest = 2**GROUPS
    window = jnp.left_shift(jnp.int32(2), head_index)
    grouped = normed.astype(jnp.float32).reshape(sequences, SEQ_LEN, width_local)
    running = jnp.cumsum(grouped, axis=1)
    padded = jnp.concatenate(
        [jnp.zeros((sequences, widest, width_local), jnp.float32), running], axis=1
    )
    lagged = lax.dynamic_slice_in_dim(padded, widest - window, SEQ_LEN, axis=1)
    position = jnp.arange(SEQ_LEN, dtype=jnp.int32)
    divisor = jnp.minimum(position + 1, window).astype(jnp.float32)
    pooled = (
        ((running - lagged) / divisor[None, :, None] - grouped)
        .astype(jnp.bfloat16)
        .reshape(tok_rows, width_local)
    )
    mixing = (
        jnp.dot(pooled, pool_weight[0], preferred_element_type=jnp.float32) * pool_scale[None, :]
    )
    gate_columns = lax.dynamic_slice_in_dim(
        gate_weight, head_index * local_heads, local_heads, axis=1
    )
    columns = lax.all_gather(normed, "tp", axis=1, tiled=True)

    flat_ids = passage_ids.reshape(-1)
    reads = flat_ids.shape[0]
    chips = lax.axis_size("st") // CORES
    chip = lax.axis_index("st") // CORES
    ids_row = jnp.pad(flat_ids, (0, 128 - reads))[None, :]
    ring_ids, both = project(ids_row, passage_gain, key_weight, value_weight, passage_store, chips)
    table, rounds = plan(ring_ids[:, 0, :reads], chip)
    kept = both.reshape(CHIP_PASSAGES, PLEN, both.shape[3])
    levels = LEVELS + (MOST_ROUNDS,)
    level = jnp.sum((rounds > jnp.array(LEVELS, jnp.int32)).astype(jnp.int32))
    branches = [
        functools.partial(ring, count, 1 + ident, reads) for ident, count in enumerate(levels)
    ]
    key_values = lax.switch(level, branches, table, kept)

    query_sum = jnp.dot(columns, query_weight, preferred_element_type=jnp.float32)
    gate_sum = jnp.dot(columns, gate_columns, preferred_element_type=jnp.float32)
    queries = query_sum.astype(jnp.bfloat16)
    gating = jax.nn.sigmoid(gate_sum)
    block_count = tok_rows // BLK
    key_values = key_values.reshape(block_count, NPB * PLEN, 2 * head_width)
    key_rows = key_values[:, :, :head_width].reshape(block_count, NPB * PLEN, local_heads, HD)
    values = key_values[:, :, head_width:].reshape(block_count, NPB * PLEN, local_heads, HD)
    query_blocks = queries.reshape(block_count, BLK, local_heads, HD)
    scores = jnp.einsum(
        "bqhd,bkhd->bhqk", query_blocks, key_rows, preferred_element_type=jnp.float32
    ) * HD ** (-0.5)
    row_max = jnp.max(scores, axis=-1, keepdims=True)
    weights = jnp.exp(scores - row_max)
    probabilities = (weights / jnp.sum(weights, axis=-1, keepdims=True)).astype(jnp.bfloat16)
    attended = jnp.einsum(
        "bhqk,bkhd->bqhd", probabilities, values, preferred_element_type=jnp.float32
    ).reshape(tok_rows, local_heads, HD)
    head_out = (attended * gating[:, :, None]).astype(jnp.bfloat16).reshape(tok_rows, head_width)
    crossed = jnp.dot(
        lax.all_gather(head_out, "tp", axis=1, tiled=True),
        out_weight, preferred_element_type=jnp.float32
    )
    return (mixing + crossed).astype(jnp.bfloat16)


def solution(mesh):
    in_specs = (
        P(("grp", "st"), "tp"),
        P(),
        P("tp", None, None),
        P("tp"),
        P(None, "tp"),
        P(),
        P(None, "tp"),
        P(None, "tp"),
        P(None, "tp"),
        P(),
        P(("grp", "st"), None, None),
        P(("grp", "st"), None),
    )
    out_specs = P(("grp", "st"), "tp")
    return jax.shard_map(
        per_device, mesh=mesh, in_specs=in_specs, out_specs=out_specs, check_vma=False
    )
```

time: 316 us -> 256 us (0.81)
  waiting for transfers between devices: 177 us -> 18.6 us
  Pallas kernels: 0 us -> 152 us
  starting transfers between devices: 42.2 us -> 0.07 us
  matrix products: 25.5 us -> 20.1 us
  local copies, waits for them, and re-layouts: 19.1 us -> 14.5 us
    pallas_call x0 -> x2, Pallas kernels: none -> 152 us  [the longest x1 115 us: ring(): pl.pallas_call(functools.partial(ring_kernel, rounds), name=f'ring_kernel...]
    all_to_all x3 -> x0, waiting for transfers between devices: 125 us -> none  [the longest x1 109 us: per_device(): lax.all_to_all(projected.reshape(st_count, capacity * PLEN, 2 * head_widt...]
    all_gather x1, waiting for transfers between devices: 52.4 us -> 0.01 us  [per_device(): columns = lax.all_gather(normed, 'tp', axis=1, tiled=True)]
    all_to_all x3 -> x0, starting transfers between devices: 42.2 us -> none  [the longest x1 24.7 us: per_device(): lax.all_to_all(request_table, 'st', split_axis=0, concat_axis=0, tiled=True)]
    all_gather x0 -> x1, waiting for transfers between devices: none -> 18.5 us  [per_device(): lax.all_gather(head_out, 'tp', axis=1, tiled=True)]
    gather x2 -> x0, local copies, waits for them, and re-layouts: 5.65 us -> none  [the longest x1 2.87 us: per_device(): jnp.take(returned.reshape(st_count * capacity, PLEN, 2 * head_width), pos...]
    convert_element_type x1 -> x0, other arithmetic: 4.43 us -> none  [normalize_rows(): return (wide_rows * inverse * passage_gain).astype(jnp.bfloat16)]
    dot_general x2 -> x1, matrix products: 6.47 us -> 2.87 us  [per_device(): jnp.dot(lax.all_gather(head_out, 'tp', axis=1, tiled=True), out_weight, p...]
  transfers between devices with their start and end apart: 4 -> 2, of which waited for: 3 -> 1; matrix products, arithmetic and copies ran while one was open for 10% -> 11% of each run, Pallas kernels for 0% -> 60%
where the time goes in v1:
time: 256 us; the launch traced here: 254 us
  Pallas kernels  152 us (59%)
  other arithmetic  23.2 us (9%)
  matrix products  20.1 us (8%)
  waiting for transfers between devices  18.6 us (7%)
  local copies, waits for them, and re-layouts  14.5 us (6%)
  between operations  14.4 us (6%)
  blocking collectives  10.9 us (4%)
    pallas_call x1, Pallas kernels, ring(): pl.pallas_call(functools.partial(ring_kernel, rounds), name=f'ring_kernel...  115 us
    pallas_call x1, Pallas kernels, project(): pl.pallas_call(project_kernel, name='project_kernel', out_shape=(jax.Shap...  36.9 us
    all_gather x1, waiting for transfers between devices, per_device(): lax.all_gather(head_out, 'tp', axis=1, tiled=True)  18.5 us
    psum x1, blocking collectives, per_device(): square_sums = lax.psum(jnp.sum(wide_tokens * wide_tokens, axis=1), 'tp')  10.9 us
    dot_general x1, matrix products, per_device(): jnp.einsum('bhqk,bkhd->bqhd', probabilities, values, preferred_element_ty...  5.65 us
  transfers between devices with their start and end apart: 2, of which 1 were waited for; matrix products, arithmetic and copies ran while one was open for 11% of the time, Pallas kernels for 60%

profile of v1, /device:TPU:40, one launch (start us, length us, event | category | flops | bytes accessed | tf_op | source)
XLA Modules:
  0.0 254.2 jit_solution(1209816153775475332)
XLA Ops:
  6.6 1.6 fusion.4
  8.2 10.9 %psum.7 = f32[1024]{0:T(1024)S(1)} all-reduce(f32[1024]{0:T(1024)S(1)} %fusion.4), channel_id=1, replica_groups=mesh['grp'=2,'st'=32,'tp'=4] {'tp'}, use_global_device_ids=true, to_apply=%region_1.0 | all-reduce | flops 1024 | bytes 8192 | tf_op jit(solution)/shard_map/psum | solution.py:306
  19.1 0.8 dynamic_slice.24
  19.9 2.5 fusion.6
  22.7 0.5 pad_bitcast_fusion.1.ids_ref
  23.3 36.9 %project_kernel.1 = (s32[16,1,128]{2,1,0:T(1,128)}, bf16[2,24,64,512]{3,2,1,0:T(8,128)(2,1)}) custom-call(s32[1,128]{1,0:T(1,128)} %pad_bitcast_fusion.1.ids_ref, f32[1,2048]{1,0:T(1,128)} %bitcast.149, bf16[2048,256]{1,0:T(8,128)(2,1)} %key_ref.1, bf16[2048,256]{1,0:T(8,128)(2,1)} %value_ref.1, bf16[24,64,2048]{2,1,0:T(8,128)(2,1)} %store_ref.1), custom_call_target="tpu_custom_call" | custom-call | flops 3221225472 | bytes 7864320 | tf_op jit(solution)/shard_map/project_kernel/pallas_call | solution.py:99
  60.2 0.7 fusion.63
  60.9 0.7 add_select_fusion.6
  61.7 0.5 convert_reduce_fusion.1
  62.3 4.6 %convert_reduce_fusion = s32[2,16,8]{2,1,0:T(8,128)S(1)} fusion(pred[2,8,16,32]{3,2,1,0:T(8,128)(4,1)S(1)} %iota_compare_fusion.3, pred[2,16,16,32]{3,2,1,0:T(8,128)(4,1)S(1)} %fusion.20), kind=kLoop, calls=%fused_computation.15 | loop fusion | flops 392960 | bytes 25600 | tf_op jit(solution)/shard_map/reduce_sum | solution.py:150
  66.9 0.4 slice_reduce_fusion
  68.4 0.1 copy.208
  68.5 0.1 copy.206
  68.6 0.1 copy.204
  68.7 0.1 copy.202
  68.8 0.1 copy.200
  68.9 0.1 copy.198
  69.0 0.1 copy.196
  69.2 0.1 stack.19
  69.5 0.6 select_reduce_fusion.5
  70.4 1.2 fusion.50
  72.3 0.1 select_reduce_fusion.3
  72.7 0.5 select_reduce_fusion
  73.3 0.1 select_reduce_fusion.2
  73.6 115.5 %conditional.1 = (bf16[32,64,512]{2,1,0:T(8,128)(2,1)S(1)}) conditional(s32[]{:T(128)} %clamp.3, (s32[3,128]{1,0:T(4,128)S(1)}, bf16[48,64,512]{2,1,0:T(8,128)(2,1)}) %tuple.70, (s32[3,128]{1,0:T(4,128)S(1)}, bf16[48,64,512]{2,1,0:T(8,128)(2,1)}) %tuple.71, (s32[3,128]{1,0:T(4,128)S(1)}, ...), branch_computations={%region_17.18_spmd, %region_18.19_spmd, %region_19.20_spmd, %regio... | conditional | flops 128000000000 | bytes 33554440 | solution.py:347
  73.8 115.1 %ring_kernel_72.1 = bf16[32,64,512]{2,1,0:T(8,128)(2,1)S(1)} custom-call(s32[3,128]{1,0:T(4,128)S(1)} %get-tuple-element.31.table_ref, bf16[48,64,512]{2,1,0:T(8,128)(2,1)} %get-tuple-element.32.kept_ref), custom_call_target="tpu_custom_call" | custom-call | flops 71999995904 | bytes 18874368 | tf_op jit(solution)/shard_map/cond/branch_0_fun/ring_kernel_72/pallas_call | solution.py:267
  189.1 1.3 copy-done.3
  190.4 2.7 %fusion.62 = (bf16[8,256,256]{2,1,0:T(8,128)(2,1)}, bf16[8,256,256]{2,1,0:T(8,128)(2,1)S(1)}) fusion(bf16[8,256,512]{2,1,0:T(8,128)(2,1)} %bitcast.123), kind=kLoop, calls=%fused_computation.179 | loop fusion | bytes 4194304 | tf_op jit(solution)/shard_map/slice | solution.py:355
  193.1 1.5 copy.219
  194.6 1.3 copy.218
  195.9 3.7 %convolution_convert_fusion = bf16[1024,256]{1,0:T(8,128)(2,1)S(1)} fusion(bf16[1024,2048]{1,0:T(8,128)(2,1)} %all-gather.3.cloned.1.call-done, bf16[2048,256]{1,0:T(8,128)(2,1)} %param.23), kind=kOutput, calls=%fused_computation.20 | convolution fusion | flops 1074003968 | bytes 5767168 | tf_op jit(solution)/shard_map/dot_general | solution.py:349
  199.6 0.1 reshape.983
  199.8 1.0 fusion.64
  200.8 1.8 fusion.17
  202.5 5.7 %convolution_bitcast_fusion = f32[8,128,2,128]{1,3,2,0:T(8,128)S(1)} fusion(bf16[8,256,2,128]{1,3,2,0:T(8,128)(2,1)} %bitcast.124, f32[8,2,128]{2,1,0:T(2,128)S(1)} %fusion.64, f32[8,2,128,256]{3,2,1,0:T(8,128)} %fusion.17), kind=kOutput, calls=%fused_computation.19 | convolution fusion | flops 136317184 | bytes 4202496 | tf_op jit(solution)/shard_map/bhqk,bkhd->bqhd/dot_general | solution.py:364
  208.2 0.6 copy.222
  208.8 3.4 %fusion.13 = f32[1024,2]{0,1:T(2,128)S(1)} fusion(bf16[1024,2048]{1,0:T(8,128)(2,1)} %all-gather.3.cloned.1.call-done, bf16[2048,8]{0,1:T(8,128)(2,1)} %param.24, s32[]{:T(128)S(6)} %select_n.238), kind=kOutput, calls=%fused_computation.24 | convolution fusion | flops 8394752 | bytes 4210692 | tf_op jit(solution)/shard_map/dot_general | solution.py:350
  212.2 1.0 fusion.14
  213.3 0.4 copy-done.1
  213.6 0.3 convert.1
  213.9 1.6 fusion.7
  215.6 1.3 copy-done.2
  216.9 2.3 broadcast_add_fusion
  219.3 1.7 copy.192
  220.9 3.3 %fusion.9 = bf16[4,256,512]{2,1,0:T(8,128)(2,1)S(1)} fusion(f32[4,256,512]{2,1,0:T(8,128)} %bitcast.117, s32[]{:T(128)S(6)} %select_n.214, f32[256]{0:T(256)S(1)} %minimum_convert_fusion, bf16[4,256,512]{2,1,0:T(8,128)(2,1)S(1)} %bitcast.116), kind=kLoop, calls=%fused_computation.16 | loop fusion | flops 2621440 | bytes 4195332 | tf_op jit(solution)/shard_map/convert_element_type | solution.py:323
  224.3 18.5 %all-gather.5.cloned.1.call-done = bf16[1024,1024]{0,1:T(8,128)(2,1)} async-done(((bf16[1024,256]{0,1:T(8,128)(2,1)}), bf16[1024,1024]{0,1:T(8,128)(2,1)}) %all-gather.5.cloned.1.call-update) | async-done | bytes 2097168 | tf_op jit(solution)/shard_map/all_gather | solution.py:369
  242.8 2.9 %fusion.67 = f32[1024,512]{1,0:T(8,128)S(1)} fusion(bf16[1024,1024]{0,1:T(8,128)(2,1)} %all-gather.5.cloned.1.call-done, bf16[1024,512]{1,0:T(8,128)(2,1)S(1)} %copy-done), kind=kOutput, calls=%fused_computation.182 | convolution fusion | flops 1073741824 | bytes 5242880 | tf_op jit(solution)/shard_map/dot_general | solution.py:368
  245.7 1.7 add_convert_fusion
  (75 shorter events, 2.7 us)
Async XLA Ops:
  6.5 236.2 %copy-start = (bf16[1024,512]{1,0:T(8,128)(2,1)S(1)}, bf16[1024,512]{1,0:T(8,128)(2,1)}, u32[]{:S(2)}) copy-start(bf16[1024,512]{1,0:T(8,128)(2,1)} %param.27) | copy-start | bytes 3145732
  6.6 189.3 %all-gather.3.cloned.1.call-start = ((), (), s32[]{:S(2)}) async-start(), calls=%async_computation | async-start | bytes 5242880 | tf_op jit(solution)/shard_map/all_gather | solution.py:332
  6.6 16.0 %copy-start.6 = (s32[8,4]{0,1:T(4,128)S(1)}, s32[8,4]{0,1:T(4,128)}, u32[]{:S(2)}) copy-start(s32[8,4]{0,1:T(4,128)} %param.30) | copy-start | bytes 388
  22.4 220.3 %all-gather.5.cloned.1.call-start = ((), (), s32[]{:S(2)}) async-start(), calls=%async_computation.1 | async-start | bytes 2621440 | tf_op jit(solution)/shard_map/all_gather | solution.py:369
  23.3 47.2 %copy-start.7 = (s32[5]{0:T(128)S(1)}, s32[5]{0:T(128)}, u32[]{:S(2)}) copy-start(s32[5]{0:T(128)} %constant.145.clone) | copy-start | bytes 64
  189.1 1.3 copy-start.3
  212.2 1.4 copy-start.1
  215.6 1.3 copy-start.2
  224.2 21.4 %copy-start.4 = (bf16[1,512,512]{2,1,0:T(8,128)(2,1)S(1)}, bf16[1,512,512]{2,1,0:T(8,128)(2,1)}, u32[]{:S(2)}) copy-start(bf16[1,512,512]{2,1,0:T(8,128)(2,1)} %param.21) | copy-start | bytes 1572868
  224.2 21.4 %copy-start.5 = (f32[512]{0:T(512)S(1)}, f32[512]{0:T(512)}, u32[]{:S(2)}) copy-start(f32[512]{0:T(512)} %param.22) | copy-start | bytes 6148
Sparse Core Ops, SparseCore 0:
  22.6 65.0 all-gather.2
  213.4 29.3 all-gather.4
